TPU v7x, 32 devices: a whole 2x2x4 slice. The times are simulated.
32 devices in a mesh: ra: 4 (over y, x), cb: 8 (over z, core).
Axes of the slice: x: 2, y: 2, z: 4, core: 2. Of those that a mesh axis runs over, the one named last changes fastest.
Arguments:
- tokens: bfloat16 [256, 4096], P(None, 'ra'), may hold values from -20 to 20, as said below
- norm_gain: float32 [2, 4096], P(None, 'ra'), may hold values from 0.1 to 1.9
- gate_weight: bfloat16 [2, 4096, 11008], P(None, 'ra', 'cb'), may hold values from -0.09375 to 0.09375
- value_weight: bfloat16 [2, 4096, 11008], P(None, 'ra', 'cb'), may hold values from -0.09375 to 0.09375
- gate_taps: float32 [2, 3, 11008], P(None, None, 'cb'), may hold values from -3.5 to 3.5
- value_taps: float32 [2, 3, 11008], P(None, None, 'cb'), may hold values from -3.5 to 3.5
- down_weight: bfloat16 [2, 11008, 4096], P(None, 'cb', 'ra'), may hold values from -0.0546875 to 0.0546875
Outputs:
- mixed: bfloat16 [256, 4096], P(None, 'ra')
Inputs may be any that keep to these rules, and one draw needn't show every extreme that they name: tokens have features drawn around zero with a scale that varies by blocks of features between about 0.3 and 3.3.
All inputs are finite; a program needn't handle non-finite values.
Results may differ from a plain program's by a relative error of at most 0.0075.
Values may be sent and summed in bfloat16 or wider, within the bound.
No kernel may reach another device: no remote copies, remote signals or barrier semaphores. Data moves between devices by JAX's collectives and lax.ppermute only.
A program may use at most 128 MiB of HBM per device.

v0:
```python
import jax
import jax.numpy as jnp
from jax import lax
from jax.sharding import PartitionSpec as P

D = 4096
epsilon = 1e-06


def conv_after(signal, earlier, kernel_taps):
    length = signal.shape[0]
    width = kernel_taps.shape[0]
    padded = jnp.concatenate([earlier, signal], axis=0)
    result = jnp.zeros(signal.shape, jnp.float32)
    for offset in range(width):
        result = result + kernel_taps[offset] * padded[offset : offset + length]
    return result


def causal_conv(signal, kernel_taps):
    width = kernel_taps.shape[0]
    return conv_after(signal, jnp.zeros((width - 1, signal.shape[1]), jnp.float32), kernel_taps)


def body(tokens, norm_gain, gate_weight, value_weight, gate_taps, value_taps, down_weight):
    stream = tokens
    for layer_index in range(gate_weight.shape[0]):
        current = stream.astype(jnp.float32)
        local_squares = jnp.sum(current * current, axis=1, keepdims=True)
        scaled = (current * norm_gain[layer_index]).astype(jnp.bfloat16)
        gate_part = jnp.dot(scaled, gate_weight[layer_index], preferred_element_type=jnp.float32)
        value_part = jnp.dot(scaled, value_weight[layer_index], preferred_element_type=jnp.float32)
        total_squares = lax.psum(local_squares, "ra")
        gate_sum, value_sum = lax.psum((gate_part, value_part), "ra")
        inverse_rms = lax.rsqrt(total_squares / D + epsilon)
        gate_conv = causal_conv(gate_sum * inverse_rms, gate_taps[layer_index])
        value_conv = causal_conv(value_sum * inverse_rms, value_taps[layer_index])
        hidden = (jax.nn.silu(gate_conv) * value_conv).astype(jnp.bfloat16)
        partial_branch = jnp.dot(
            hidden, down_weight[layer_index], preferred_element_type=jnp.float32
        )
        branch = lax.psum(partial_branch, "cb")
        stream = (0.5 * current + branch).astype(jnp.bfloat16)
    return stream


def solution(mesh):
    return jax.shard_map(
        body,
        mesh=mesh,
        in_specs=(
            P(None, "ra"),
            P(None, "ra"),
            P(None, "ra", "cb"),
            P(None, "ra", "cb"),
            P(None, None, "cb"),
            P(None, None, "cb"),
            P(None, "cb", "ra"),
        ),
        out_specs=P(None, "ra"),
        check_vma=False,
    )
```

profile of v0, /device:TPU:0, one launch (start us, length us, event | category | flops | bytes accessed | tf_op | source)
XLA Modules:
  0.0 333.7 jit_solution(11090075387825171046)
XLA Ops:
  6.5 0.0 all-reduce.17.cloned.1.call-start
  6.5 0.8 fusion.57
  7.3 0.0 copy-start
  7.3 4.0 %fusion.8 = f32[256,1376]{0,1:T(8,128)} fusion(bf16[2,1024,1376]{1,2,0:T(8,128)(2,1)} %param.10, bf16[256,1024]{1,0:T(8,128)(2,1)} %param.7, f32[1024]{0:T(1024)S(1)} %bitcast.30), kind=kOutput, calls=%fused_computation.8 | convolution fusion | flops 722206720 | bytes 4755456 | tf_op jit(solution)/shard_map/dot_general | solution.py:32
  11.4 0.0 copy-done
  11.4 3.8 %fusion.10 = f32[256,1376]{0,1:T(8,128)} fusion(bf16[2,1024,1376]{1,2,0:T(8,128)(2,1)} %param.9, bf16[256,1024]{1,0:T(8,128)(2,1)S(1)} %copy-done, f32[1024]{0:T(1024)S(1)} %bitcast.31), kind=kOutput, calls=%fused_computation.10 | convolution fusion | flops 722206720 | bytes 4755456 | tf_op jit(solution)/shard_map/dot_general | solution.py:31
  15.2 0.0 copy-start.1
  15.2 0.0 copy-start.2
  15.2 0.0 all-reduce.17.cloned.1.call-update
  15.2 0.0 all-reduce.11.cloned.1.call-start
  15.3 0.2 fusion.41
  15.5 11.5 %psum.57 = f32[256,1]{0,1:T(1,128)S(1)} all-reduce(f32[256,1]{0,1:T(1,128)S(1)} %bitcast.27), channel_id=1, replica_groups=mesh['ra'=4,'cb'=8] {'ra'}, use_global_device_ids=true, to_apply=%region_2.0 | all-reduce | flops 256 | bytes 2048 | tf_op jit(solution)/shard_map/psum | solution.py:33
  27.0 0.0 copy-done.1
  27.0 0.0 copy-done.2
  27.0 0.2 slice_reduce_fusion.2
  27.1 72.5 %all-reduce.17.cloned.1.call-done = (f32[256,1376]{0,1:T(8,128)}, f32[256,1376]{0,1:T(8,128)}) async-done(((f32[256,1376]{0,1:T(8,128)}, f32[256,1376]{0,1:T(8,128)}), (f32[256,1376]{0,1:T(8,128)}, f32[256,1376]{0,1:T(8,128)})) %all-reduce.17.cloned.1.call-update) | async-done | bytes 2818064 | tf_op jit(solution)/shard_map/psum | solution.py:34
  99.6 2.0 broadcast_multiply_fusion.3
  101.6 6.3 %fusion.6 = f32[256,1024]{1,0:T(8,128)} fusion(bf16[2,1376,1024]{2,1,0:T(8,128)(2,1)} %param.13, f32[256,1376]{0,1:T(8,128)S(1)} %get-tuple-element.28, f32[256,1376]{0,1:T(8,128)S(1)} %get-tuple-element.27, f32[1376]{0:T(1024)S(1)} %get-tuple-element.12, f32[1376]{0:T(1024)S(1)} %get-tuple-element.13, f32[1376]{0:T(1024)S(1)} %get-tuple-element.14, ...), kind=kOutput, calls=%fused_computation.6 | convolution fusion | flops 727056384 | bytes 6717696 | tf_op jit(solution)/shard_map/dot_general | solution.py:39
  107.9 0.0 all-reduce.11.cloned.1.call-update
  107.9 0.0 all-reduce.15.cloned.1.call-start
  107.9 59.4 %all-reduce.11.cloned.1.call-done = f32[256,1024]{1,0:T(8,128)} async-done(((f32[256,1024]{1,0:T(8,128)}), f32[256,1024]{1,0:T(8,128)}) %all-reduce.11.cloned.1.call-update) | async-done | bytes 1048592 | tf_op jit(solution)/shard_map/psum | solution.py:42
  167.3 1.5 fusion.45
  168.8 3.8 %fusion.4 = f32[256,1376]{0,1:T(8,128)} fusion(bf16[2,1024,1376]{1,2,0:T(8,128)(2,1)} %param.9, bf16[256,1024]{1,0:T(8,128)(2,1)S(1)} %get-tuple-element.22, f32[1024]{0:T(1024)S(1)} %bitcast.28), kind=kOutput, calls=%fused_computation.4 | convolution fusion | flops 722206720 | bytes 4755456 | tf_op jit(solution)/shard_map/dot_general | solution.py:31
  172.6 3.8 %fusion.2 = f32[256,1376]{0,1:T(8,128)} fusion(bf16[2,1024,1376]{1,2,0:T(8,128)(2,1)} %param.10, bf16[256,1024]{1,0:T(8,128)(2,1)S(1)} %get-tuple-element.22, f32[1024]{0:T(1024)S(1)} %bitcast.29), kind=kOutput, calls=%fused_computation.2 | convolution fusion | flops 722206720 | bytes 4755456 | tf_op jit(solution)/shard_map/dot_general | solution.py:32
  176.5 0.0 all-reduce.15.cloned.1.call-update
  176.5 0.0 all-reduce.13.cloned.1.call-start
  176.5 10.1 %psum.61 = f32[256,1]{0,1:T(1,128)S(1)} all-reduce(f32[256,1]{0,1:T(1,128)S(1)} %bitcast.24), channel_id=1, replica_groups=mesh['ra'=4,'cb'=8] {'ra'}, use_global_device_ids=true, to_apply=%region_7.8 | all-reduce | flops 256 | bytes 2048 | tf_op jit(solution)/shard_map/psum | solution.py:33
  186.6 70.6 %all-reduce.15.cloned.1.call-done = (f32[256,1376]{0,1:T(8,128)}, f32[256,1376]{0,1:T(8,128)}) async-done(((f32[256,1376]{0,1:T(8,128)}, f32[256,1376]{0,1:T(8,128)}), (f32[256,1376]{0,1:T(8,128)}, f32[256,1376]{0,1:T(8,128)})) %all-reduce.15.cloned.1.call-update) | async-done | bytes 2818064 | tf_op jit(solution)/shard_map/psum | solution.py:34
  257.3 2.0 broadcast_multiply_fusion.1
  259.2 6.3 %fusion = f32[256,1024]{1,0:T(8,128)} fusion(bf16[2,1376,1024]{2,1,0:T(8,128)(2,1)} %param.13, f32[256,1376]{0,1:T(8,128)S(1)} %get-tuple-element.26, f32[256,1376]{0,1:T(8,128)S(1)} %get-tuple-element.25, f32[1376]{0:T(1024)S(1)} %get-tuple-element.15, f32[1376]{0:T(1024)S(1)} %get-tuple-element.16, f32[1376]{0:T(1024)S(1)} %get-tuple-element.11, ...), kind=kOutput, calls=%fused_computation | convolution fusion | flops 727056384 | bytes 6717696 | tf_op jit(solution)/shard_map/dot_general | solution.py:39
  265.5 0.0 all-reduce.13.cloned.1.call-update
  265.5 59.4 %all-reduce.13.cloned.1.call-done = f32[256,1024]{1,0:T(8,128)} async-done(((f32[256,1024]{1,0:T(8,128)}), f32[256,1024]{1,0:T(8,128)}) %all-reduce.13.cloned.1.call-update) | async-done | bytes 1048592 | tf_op jit(solution)/shard_map/psum | solution.py:42
  324.9 2.2 fusion.43
  (2 shorter events, 0.0 us)
Async XLA Ops:
  6.5 93.1 %all-reduce.17.cloned.1.call-start = ((), (), s32[]{:S(2)}) async-start(), calls=%async_computation.3 | async-start | bytes 5636096 | tf_op jit(solution)/shard_map/psum | solution.py:34
  7.3 4.0 %copy-start = (bf16[256,1024]{1,0:T(8,128)(2,1)S(1)}, bf16[256,1024]{1,0:T(8,128)(2,1)}, u32[]{:S(2)}) copy-start(bf16[256,1024]{1,0:T(8,128)(2,1)} %param.7) | copy-start | bytes 1572868
  15.2 11.8 %copy-start.1 = (f32[2,3,1376]{2,0,1:T(2,128)S(1)}, f32[2,3,1376]{2,0,1:T(2,128)}, u32[]{:S(2)}) copy-start(f32[2,3,1376]{2,0,1:T(2,128)} %param.12) | copy-start | bytes 99076
  15.2 11.8 %copy-start.2 = (f32[2,3,1376]{2,0,1:T(2,128)S(1)}, f32[2,3,1376]{2,0,1:T(2,128)}, u32[]{:S(2)}) copy-start(f32[2,3,1376]{2,0,1:T(2,128)} %param.11) | copy-start | bytes 99076
  15.2 152.1 %all-reduce.11.cloned.1.call-start = ((), (), s32[]{:S(2)}) async-start(), calls=%async_computation | async-start | bytes 2097152 | tf_op jit(solution)/shard_map/psum | solution.py:42
  107.9 149.4 %all-reduce.15.cloned.1.call-start = ((), (), s32[]{:S(2)}) async-start(), calls=%async_computation.2 | async-start | bytes 5636096 | tf_op jit(solution)/shard_map/psum | solution.py:34
  176.5 148.4 %all-reduce.13.cloned.1.call-start = ((), (), s32[]{:S(2)}) async-start(), calls=%async_computation.1 | async-start | bytes 2097152 | tf_op jit(solution)/shard_map/psum | solution.py:42
Sparse Core Ops, SparseCore 0:
  15.3 84.2 all-reduce.16
  108.0 59.2 all-reduce.10
  176.6 80.6 all-reduce.14
  265.6 59.2 all-reduce.12
where the time goes:
time: 334 us
  waiting for transfers between devices  262 us (78%)
  matrix products  28 us (8%)
  blocking collectives  21.6 us (6%)
  between operations  13.2 us (4%)
  other arithmetic  7.81 us (2%)
    psum x2, waiting for transfers between devices, body(): gate_sum, value_sum = lax.psum((gate_part, value_part), 'ra')  143 us
    psum x2, waiting for transfers between devices, body(): branch = lax.psum(partial_branch, 'cb')  119 us
    psum x2, blocking collectives, body(): total_squares = lax.psum(local_squares, 'ra')  21.6 us
    dot_general x2, matrix products, body(): jnp.dot(hidden, down_weight[layer_index], preferred_element_type=jnp.floa...  12.5 us
    dot_general x2, matrix products, body(): jnp.dot(scaled, value_weight[layer_index], preferred_element_type=jnp.flo...  7.86 us
    dot_general x2, matrix products, body(): jnp.dot(scaled, gate_weight[layer_index], preferred_element_type=jnp.floa...  7.65 us
  transfers between devices with their start and end apart: 4, of which 4 were waited for; matrix products, arithmetic and copies ran while one was open for 0% of the time, Pallas kernels for 0%

commit v1 on v0

--- a/solution.py
+++ b/solution.py
@@ -39,7 +39,9 @@
         partial_branch = jnp.dot(
             hidden, down_weight[layer_index], preferred_element_type=jnp.float32
         )
-        branch = lax.psum(partial_branch, "cb")
+        branch = partial_branch
+        for hop in (1, 2, 4):
+            branch = branch + lax.ppermute(branch, "cb", [(dev, dev ^ hop) for dev in range(8)])
         stream = (0.5 * current + branch).astype(jnp.bfloat16)
     return stream
 

time: 334 us -> 361 us (1.081)
  waiting for transfers between devices: 262 us -> 288 us
  starting transfers between devices: 0.13 us -> 8.24 us
  matrix products: 28 us -> 22.5 us
    ppermute x0 -> x6, waiting for transfers between devices: none -> 143 us  [body(): lax.ppermute(branch, 'cb', [(dev, dev ^ hop) for dev in range(8)])]
    psum x2 -> x0, waiting for transfers between devices: 119 us -> none  [body(): branch = lax.psum(partial_branch, 'cb')]
    ppermute x0 -> x6, starting transfers between devices: none -> 8.19 us  [body(): lax.ppermute(branch, 'cb', [(dev, dev ^ hop) for dev in range(8)])]
  transfers between devices with their start and end apart: 4 -> 8, of which waited for: 4 -> 8; matrix products, arithmetic and copies ran while one was open for 0% -> 0% of each run, Pallas kernels for 0% -> 0%
where the time goes in v1:
time: 361 us
  waiting for transfers between devices  288 us (80%)
  matrix products  22.5 us (6%)
  blocking collectives  20.7 us (6%)
  between operations  13.5 us (4%)
  starting transfers between devices  8.24 us (2%)
  other arithmetic  6.37 us (2%)
    psum x2, waiting for transfers between devices, body(): gate_sum, value_sum = lax.psum((gate_part, value_part), 'ra')  145 us
    ppermute x6, waiting for transfers between devices, body(): lax.ppermute(branch, 'cb', [(dev, dev ^ hop) for dev in range(8)])  143 us
    psum x2, blocking collectives, body(): total_squares = lax.psum(local_squares, 'ra')  20.7 us
    dot_general x2, matrix products, body(): jnp.dot(hidden, down_weight[layer_index], preferred_element_type=jnp.floa...  10.5 us
    ppermute x6, starting transfers between devices, body(): lax.ppermute(branch, 'cb', [(dev, dev ^ hop) for dev in range(8)])  8.19 us
  transfers between devices with their start and end apart: 8, of which 8 were waited for; matrix products, arithmetic and copies ran while one was open for 0% of the time, Pallas kernels for 0%

profile of v1, /device:TPU:0, one launch (start us, length us, event | category | flops | bytes accessed | tf_op | source)
XLA Modules:
  0.0 360.6 jit_solution(11903880196491729193)
XLA Ops:
  6.5 0.0 all-reduce.11.cloned.1.call-start
  6.5 0.8 fusion.57
  7.3 0.0 copy-start
  7.3 4.0 %fusion.8 = f32[256,1376]{0,1:T(8,128)} fusion(bf16[2,1024,1376]{1,2,0:T(8,128)(2,1)} %param.10, bf16[256,1024]{1,0:T(8,128)(2,1)} %param.7, f32[1024]{0:T(1024)S(1)} %bitcast.30), kind=kOutput, calls=%fused_computation.8 | convolution fusion | flops 722206720 | bytes 4755456 | tf_op jit(solution)/shard_map/dot_general | solution.py:32
  11.4 0.0 copy-done
  11.4 3.8 %fusion.10 = f32[256,1376]{0,1:T(8,128)} fusion(bf16[2,1024,1376]{1,2,0:T(8,128)(2,1)} %param.9, bf16[256,1024]{1,0:T(8,128)(2,1)S(1)} %copy-done, f32[1024]{0:T(1024)S(1)} %bitcast.31), kind=kOutput, calls=%fused_computation.10 | convolution fusion | flops 722206720 | bytes 4755456 | tf_op jit(solution)/shard_map/dot_general | solution.py:31
  15.2 0.0 copy-start.1
  15.2 0.0 all-reduce.11.cloned.1.call-update
  15.2 0.0 all-reduce.9.cloned.1.call-start
  15.3 0.2 fusion.41
  15.5 11.5 %psum.43 = f32[256,1]{0,1:T(1,128)S(1)} all-reduce(f32[256,1]{0,1:T(1,128)S(1)} %bitcast.27), channel_id=1, replica_groups=mesh['ra'=4,'cb'=8] {'ra'}, use_global_device_ids=true, to_apply=%region_2.0 | all-reduce | flops 256 | bytes 2048 | tf_op jit(solution)/shard_map/psum | solution.py:33
  26.9 0.0 copy-done.1
  26.9 0.0 copy-done.2
  26.9 0.2 slice_reduce_fusion.2
  27.1 72.5 %all-reduce.11.cloned.1.call-done = (f32[256,1376]{0,1:T(8,128)}, f32[256,1376]{0,1:T(8,128)}) async-done(((f32[256,1376]{0,1:T(8,128)}, f32[256,1376]{0,1:T(8,128)}), (f32[256,1376]{0,1:T(8,128)}, f32[256,1376]{0,1:T(8,128)})) %all-reduce.11.cloned.1.call-update) | async-done | bytes 2818064 | tf_op jit(solution)/shard_map/psum | solution.py:34
  99.6 2.1 broadcast_multiply_fusion.3
  101.8 0.0 slice-start.1
  101.8 5.3 %fusion.6 = f32[256,1024]{1,0:T(8,128)S(1)} fusion(bf16[2,1376,1024]{2,1,0:T(8,128)(2,1)} %param.13, f32[256,1376]{0,1:T(8,128)S(1)} %get-tuple-element.28, f32[256,1376]{0,1:T(8,128)S(1)} %get-tuple-element.27, f32[1376]{0:T(1024)S(1)} %get-tuple-element.12, f32[1376]{0:T(1024)S(1)} %get-tuple-element.13, f32[1376]{0:T(1024)S(1)} %get-tuple-element.14, ...), kind=kOutput, calls=%fused_computation.6 | convolution fusion | flops 727056384 | bytes 6717696 | tf_op jit(solution)/shard_map/dot_general | solution.py:39
  107.1 0.1 collective-permute-start
  107.2 2.6 collective-permute-done
  109.8 0.2 add.87
  110.0 1.5 collective-permute-start.1
  111.6 23.7 %collective-permute-done.1 = f32[256,1024]{1,0:T(8,128)S(1)} collective-permute-done((f32[256,1024]{1,0:T(8,128)S(1)}, f32[256,1024]{1,0:T(8,128)S(1)}, u32[]{:S(2)}, u32[]{:S(2)}) %collective-permute-start.1) | collective-permute-done | bytes 1048608 | tf_op jit(solution)/shard_map/ppermute | solution.py:44
  135.3 0.2 add.88
  135.4 0.0 slice-start.3
  135.5 2.5 collective-permute-start.2
  137.9 45.3 %collective-permute-done.2 = f32[256,1024]{1,0:T(8,128)S(1)} collective-permute-done((f32[256,1024]{1,0:T(8,128)S(1)}, f32[256,1024]{1,0:T(8,128)S(1)}, u32[]{:S(2)}, u32[]{:S(2)}) %collective-permute-start.2) | collective-permute-done | bytes 1048608 | tf_op jit(solution)/shard_map/ppermute | solution.py:44
  183.2 0.3 fusion.45
  183.6 0.0 slice-done
  183.6 0.0 slice-done.1
  183.6 2.0 fusion.4
  185.6 0.0 slice-done.2
  185.6 0.0 slice-done.3
  185.6 2.0 fusion.2
  187.7 0.0 all-reduce.9.cloned.1.call-update
  187.7 9.2 %psum.46 = f32[256,1]{0,1:T(1,128)S(1)} all-reduce(f32[256,1]{0,1:T(1,128)S(1)} %bitcast.24), channel_id=1, replica_groups=mesh['ra'=4,'cb'=8] {'ra'}, use_global_device_ids=true, to_apply=%region_6.7 | all-reduce | flops 256 | bytes 2048 | tf_op jit(solution)/shard_map/psum | solution.py:33
  196.9 72.4 %all-reduce.9.cloned.1.call-done = (f32[256,1376]{0,1:T(8,128)}, f32[256,1376]{0,1:T(8,128)}) async-done(((f32[256,1376]{0,1:T(8,128)}, f32[256,1376]{0,1:T(8,128)}), (f32[256,1376]{0,1:T(8,128)}, f32[256,1376]{0,1:T(8,128)})) %all-reduce.9.cloned.1.call-update) | async-done | bytes 2818064 | tf_op jit(solution)/shard_map/psum | solution.py:34
  269.4 2.0 broadcast_multiply_fusion.1
  271.3 5.2 %fusion = f32[256,1024]{1,0:T(8,128)S(1)} fusion(bf16[2,1376,1024]{2,1,0:T(8,128)(2,1)} %param.13, f32[256,1376]{0,1:T(8,128)S(1)} %get-tuple-element.26, f32[256,1376]{0,1:T(8,128)S(1)} %get-tuple-element.25, f32[1376]{0:T(1024)S(1)} %get-tuple-element.15, f32[1376]{0:T(1024)S(1)} %get-tuple-element.16, f32[1376]{0:T(1024)S(1)} %get-tuple-element.11, ...), kind=kOutput, calls=%fused_computation | convolution fusion | flops 727056384 | bytes 6717696 | tf_op jit(solution)/shard_map/dot_general | solution.py:39
  276.5 0.1 collective-permute-start.3
  276.6 2.6 collective-permute-done.3
  279.3 0.2 add.97
  279.4 1.6 collective-permute-start.4
  281.0 23.7 %collective-permute-done.4 = f32[256,1024]{1,0:T(8,128)S(1)} collective-permute-done((f32[256,1024]{1,0:T(8,128)S(1)}, f32[256,1024]{1,0:T(8,128)S(1)}, u32[]{:S(2)}, u32[]{:S(2)}) %collective-permute-start.4) | collective-permute-done | bytes 1048608 | tf_op jit(solution)/shard_map/ppermute | solution.py:44
  304.7 0.2 add.98
  304.9 2.5 collective-permute-start.5
  307.3 45.3 %collective-permute-done.5 = f32[256,1024]{1,0:T(8,128)S(1)} collective-permute-done((f32[256,1024]{1,0:T(8,128)S(1)}, f32[256,1024]{1,0:T(8,128)S(1)}, u32[]{:S(2)}, u32[]{:S(2)}) %collective-permute-start.5) | collective-permute-done | bytes 1048608 | tf_op jit(solution)/shard_map/ppermute | solution.py:44
  352.7 1.1 fusion.43
  (7 shorter events, 0.0 us)
Async XLA Ops:
  6.5 93.1 %all-reduce.11.cloned.1.call-start = ((), (), s32[]{:S(2)}) async-start(), calls=%async_computation.1 | async-start | bytes 5636096 | tf_op jit(solution)/shard_map/psum | solution.py:34
  7.3 4.0 %copy-start = (bf16[256,1024]{1,0:T(8,128)(2,1)S(1)}, bf16[256,1024]{1,0:T(8,128)(2,1)}, u32[]{:S(2)}) copy-start(bf16[256,1024]{1,0:T(8,128)(2,1)} %param.7) | copy-start | bytes 1572868
  15.2 11.8 %copy-start.1 = (f32[2,3,1376]{2,0,1:T(2,128)S(1)}, f32[2,3,1376]{2,0,1:T(2,128)}, u32[]{:S(2)}) copy-start(f32[2,3,1376]{2,0,1:T(2,128)} %param.12) | copy-start | bytes 99076
  15.2 11.8 %copy-start.2 = (f32[2,3,1376]{2,0,1:T(2,128)S(1)}, f32[2,3,1376]{2,0,1:T(2,128)}, u32[]{:S(2)}) copy-start(f32[2,3,1376]{2,0,1:T(2,128)} %param.11) | copy-start | bytes 99076
  15.2 254.1 %all-reduce.9.cloned.1.call-start = ((), (), s32[]{:S(2)}) async-start(), calls=%async_computation | async-start | bytes 5636096 | tf_op jit(solution)/shard_map/psum | solution.py:34
  99.6 83.9 %slice-start = ((s8[5636096]{0:T(1024)(128)(4,1)}), s8[4194304]{0:T(1024)(128)(4,1)S(1)}, s32[]{:S(2)}) async-start(s8[5636096]{0:T(1024)(128)(4,1)} %bitcast.32), calls=%async_computation.2 | async-start | bytes 8388608
  101.8 81.8 %slice-start.1 = ((s8[5636096]{0:T(1024)(128)(4,1)}), s8[1441792]{0:T(1024)(128)(4,1)S(1)}, s32[]{:S(2)}) async-start(s8[5636096]{0:T(1024)(128)(4,1)} %bitcast.32), calls=%async_computation.3 | async-start | bytes 2883584
  107.1 2.7 collective-permute-start
  110.0 25.3 %collective-permute-start.1 = (f32[256,1024]{1,0:T(8,128)S(1)}, f32[256,1024]{1,0:T(8,128)S(1)}, u32[]{:S(2)}, u32[]{:S(2)}) collective-permute-start(f32[256,1024]{1,0:T(8,128)S(1)} %add.87), channel_id=1, source_target_pairs={{0,2},{1,3},{2,0},{3,1},{4,6},{5,7},{6,4},{7,5},{8,10},{9,11},{10,... | collective-permute-start | bytes 3145736 | tf_op jit(solution)/shard_map/ppermute | solution.py:44
  135.3 50.4 %slice-start.2 = ((s8[5636096]{0:T(1024)(128)(4,1)}), s8[4194304]{0:T(1024)(128)(4,1)S(1)}, s32[]{:S(2)}) async-start(s8[5636096]{0:T(1024)(128)(4,1)} %bitcast.34), calls=%async_computation.4 | async-start | bytes 8388608
  135.4 50.2 %slice-start.3 = ((s8[5636096]{0:T(1024)(128)(4,1)}), s8[1441792]{0:T(1024)(128)(4,1)S(1)}, s32[]{:S(2)}) async-start(s8[5636096]{0:T(1024)(128)(4,1)} %bitcast.34), calls=%async_computation.5 | async-start | bytes 2883584
  135.5 47.8 %collective-permute-start.2 = (f32[256,1024]{1,0:T(8,128)S(1)}, f32[256,1024]{1,0:T(8,128)S(1)}, u32[]{:S(2)}, u32[]{:S(2)}) collective-permute-start(f32[256,1024]{1,0:T(8,128)S(1)} %add.88), channel_id=1, source_target_pairs={{0,4},{1,5},{2,6},{3,7},{4,0},{5,1},{6,2},{7,3},{8,12},{9,13},{10,... | collective-permute-start | bytes 3145736 | tf_op jit(solution)/shard_map/ppermute | solution.py:44
  276.5 2.7 collective-permute-start.3
  279.4 25.3 %collective-permute-start.4 = (f32[256,1024]{1,0:T(8,128)S(1)}, f32[256,1024]{1,0:T(8,128)S(1)}, u32[]{:S(2)}, u32[]{:S(2)}) collective-permute-start(f32[256,1024]{1,0:T(8,128)S(1)} %add.97), channel_id=1, source_target_pairs={{0,2},{1,3},{2,0},{3,1},{4,6},{5,7},{6,4},{7,5},{8,10},{9,11},{10,... | collective-permute-start | bytes 3145736 | tf_op jit(solution)/shard_map/ppermute | solution.py:44
  304.9 47.8 %collective-permute-start.5 = (f32[256,1024]{1,0:T(8,128)S(1)}, f32[256,1024]{1,0:T(8,128)S(1)}, u32[]{:S(2)}, u32[]{:S(2)}) collective-permute-start(f32[256,1024]{1,0:T(8,128)S(1)} %add.98), channel_id=1, source_target_pairs={{0,4},{1,5},{2,6},{3,7},{4,0},{5,1},{6,2},{7,3},{8,12},{9,13},{10,... | collective-permute-start | bytes 3145736 | tf_op jit(solution)/shard_map/ppermute | solution.py:44
Sparse Core Ops, SparseCore 0:
  15.3 84.2 all-reduce.10
  187.8 81.4 all-reduce.8
